TPU v7x, 32 devices: a whole 2x2x4 slice. The times are simulated.
32 devices in a mesh: ep: 8 (over z, y), tp: 4 (over x, core).
Axes of the slice: x: 2, y: 2, z: 4, core: 2. Of those that a mesh axis runs over, the one named last changes fastest.
Arguments:
- tokens: bfloat16 [64, 1024], P('ep'), may hold values from -6 to 6
- mix_gain: float32 [1024], replicated, may hold values from 0.1 to 1.9
- w_query: bfloat16 [1024, 512], P(None, 'tp'), may hold values from -0.1875 to 0.1875
- w_key: bfloat16 [1024, 512], P(None, 'tp'), may hold values from -0.1875 to 0.1875
- w_value: bfloat16 [1024, 1024], P(None, 'tp'), may hold values from -0.1875 to 0.1875
- w_ogate: bfloat16 [1024, 1024], P(None, 'tp'), may hold values from -0.1875 to 0.1875
- w_igate: bfloat16 [1024, 4], replicated, may hold values from -0.1875 to 0.1875
- w_fgate: bfloat16 [1024, 4], replicated, may hold values from -0.1875 to 0.1875
- forget_bias: float32 [4], replicated, may hold values from -1 to 3
- head_gain: float32 [1024], P('tp'), may hold values from 0.1 to 1.9
- w_out: bfloat16 [1024, 1024], P('tp'), may hold values from -0.1875 to 0.1875
- memory: float32 [64, 4, 128, 256], P('ep', 'tp'), may hold values from -0.4 to 0.4
- normalizer: float32 [64, 4, 128], P('ep', 'tp'), may hold values from -0.4 to 0.4
- running_max: float32 [64, 4], P('ep', 'tp'), may hold values from -4 to 4
- ffn_gain: float32 [1024], replicated, may hold values from 0.1 to 1.9
- route: int32 [64, 2], replicated, may hold values from 0 to 7, all different within a row; in each aligned block of 64 rows (0 to 63, 64 to 127, ...) at most 32 rows name the same one
- route_weight: float32 [64, 2], replicated, may hold values from 0.05 to 1
- w_gate: bfloat16 [8, 1024, 512], P('ep', None, 'tp'), may hold values from -0.1875 to 0.1875
- w_up: bfloat16 [8, 1024, 512], P('ep', None, 'tp'), may hold values from -0.1875 to 0.1875
- w_down: bfloat16 [8, 512, 1024], P('ep', 'tp'), may hold values from -0.25 to 0.25
Outputs:
- mixed: bfloat16 [64, 1024], P(None, 'ep')
- new_memory: float32 [64, 4, 128, 256], P('ep', 'tp')
- new_normalizer: float32 [64, 4, 128], P('ep', 'tp')
- new_max: float32 [64, 4], P('ep', 'tp')
Inputs may be any that keep to these rules, and one draw needn't show every extreme that they name: `route`: each expert is named by at most 32 routes in all, a bound that some block reaches; the two choices of a token differ.
All inputs are finite; a program needn't handle non-finite values.
Results may differ from a plain program's by a relative error of at most 0.014.
Values may be sent and summed in bfloat16 or wider, within the bound.
No kernel may reach another device: no remote copies, remote signals or barrier semaphores. Data moves between devices by JAX's collectives and lax.ppermute only.
A program may use at most 64 MiB of HBM per device.

v0:
```python
import jax
import jax.numpy as jnp
from jax import lax
from jax.sharding import PartitionSpec as P

EXPERT_CAPACITY = 32
EPS = 1e-06


def round_trip(values):
    rounded = lax.optimization_barrier(values.astype(jnp.bfloat16))
    return rounded.astype(jnp.float32)


def norm_rows(values, gain):
    floats = values.astype(jnp.float32)
    scale = lax.rsqrt(jnp.mean(floats * floats, axis=-1, keepdims=True) + EPS)
    return (floats * scale * gain).astype(jnp.bfloat16)


def slot_targets(route, expert_count, capacity):
    flat = route.reshape(-1)
    onehot = (flat[:, None] == jnp.arange(expert_count, dtype=jnp.int32)[None, :]).astype(jnp.int32)
    before = jnp.cumsum(onehot, axis=0) - onehot
    slot = jnp.sum(before * onehot, axis=1)
    return flat * capacity + slot


def shards(
    tokens,
    mix_gain,
    w_query,
    w_key,
    w_value,
    w_ogate,
    w_igate,
    w_fgate,
    forget_bias,
    head_gain,
    w_out,
    memory,
    normalizer,
    running_max,
    ffn_gain,
    route,
    route_weight,
    w_gate,
    w_up,
    w_down,
):
    width = tokens.shape[1]
    col_count = width // lax.axis_size("ep")
    qk_dim = w_query.shape[1]
    normed = norm_rows(tokens, mix_gain)
    query = round_trip(jnp.dot(normed, w_query, preferred_element_type=jnp.float32))
    scaled_key = round_trip(
        jnp.dot(normed, w_key, preferred_element_type=jnp.float32)
    ) * qk_dim ** (-0.5)
    value = round_trip(jnp.dot(normed, w_value, preferred_element_type=jnp.float32))
    ogate = round_trip(jnp.dot(normed, w_ogate, preferred_element_type=jnp.float32))
    head_pick = (jnp.arange(w_igate.shape[1], dtype=jnp.int32) == lax.axis_index("tp")).astype(
        jnp.float32
    )
    log_in = jnp.sum(
        jnp.dot(normed, w_igate, preferred_element_type=jnp.float32) * head_pick, axis=1
    )
    forget_pre = jnp.sum(
        jnp.dot(normed, w_fgate, preferred_element_type=jnp.float32) * head_pick, axis=1
    )
    log_forget = jax.nn.log_sigmoid(forget_pre + jnp.sum(forget_bias * head_pick))
    old_max = running_max[:, 0]
    new_max = jnp.maximum(log_forget + old_max, log_in)
    keep = jnp.exp(log_forget + old_max - new_max)
    admit = jnp.exp(log_in - new_max)
    state = (
        keep[:, None, None] * memory[:, 0]
        + admit[:, None, None] * scaled_key[:, :, None] * value[:, None, :]
    )
    norm_state = keep[:, None] * normalizer[:, 0] + admit[:, None] * scaled_key
    numer = jnp.einsum("tk,tkv->tv", query, state, precision=lax.Precision.HIGHEST)
    denom = jnp.sum(query * norm_state, axis=1)
    read = numer / jnp.maximum(jnp.abs(denom), jnp.exp(-new_max))[:, None]
    scale = lax.rsqrt(jnp.mean(read * read, axis=-1, keepdims=True) + EPS)
    gated = (jax.nn.sigmoid(ogate) * read * scale * head_gain).astype(jnp.bfloat16)
    local_output = lax.psum(
        jnp.dot(gated, w_out, preferred_element_type=jnp.float32).astype(jnp.bfloat16), "tp"
    ).astype(jnp.float32)
    middle_rows = (tokens.astype(jnp.float32) + local_output).astype(jnp.bfloat16)
    middle = lax.all_to_all(middle_rows, "ep", split_axis=1, concat_axis=0, tiled=True)
    expert_count = w_gate.shape[0] * lax.axis_size("ep")
    topk_count = route.shape[1]
    targets = slot_targets(route, expert_count, EXPERT_CAPACITY)
    buffer = (
        jnp.zeros((expert_count * EXPERT_CAPACITY, col_count), jnp.bfloat16)
        .at[targets]
        .set(jnp.repeat(middle, topk_count, axis=0))
    )
    buffer = buffer.reshape(expert_count, EXPERT_CAPACITY, col_count)
    rows = lax.all_to_all(buffer, "ep", split_axis=0, concat_axis=2, tiled=True)
    rows = norm_rows(rows, ffn_gain)
    gate_v = jnp.einsum("ecd,edf->ecf", rows, w_gate, preferred_element_type=jnp.float32)
    up_v = jnp.einsum("ecd,edf->ecf", rows, w_up, preferred_element_type=jnp.float32)
    activation = (jax.nn.silu(gate_v) * up_v).astype(jnp.bfloat16)
    partial_value = jnp.einsum(
        "ecf,efd->ecd", activation, w_down, preferred_element_type=jnp.float32
    )
    results = lax.psum(partial_value.astype(jnp.bfloat16), "tp")
    returned = lax.all_to_all(results, "ep", split_axis=2, concat_axis=0, tiled=True)
    picked = returned.reshape(expert_count * EXPERT_CAPACITY, col_count)[targets]
    picked = picked.reshape(route.shape[0], topk_count, col_count).astype(jnp.float32)
    weights = route_weight / jnp.sum(route_weight, axis=1, keepdims=True)
    mixed = (middle.astype(jnp.float32) + jnp.sum(picked * weights[:, :, None], axis=1)).astype(
        jnp.bfloat16
    )
    return (mixed, state[:, None], norm_state[:, None], new_max[:, None])


def solution(mesh):
    return jax.shard_map(
        shards,
        mesh=mesh,
        in_specs=(
            P("ep", None),
            P(),
            P(None, "tp"),
            P(None, "tp"),
            P(None, "tp"),
            P(None, "tp"),
            P(),
            P(),
            P(),
            P("tp"),
            P("tp", None),
            P("ep", "tp", None, None),
            P("ep", "tp", None),
            P("ep", "tp"),
            P(),
            P(),
            P(),
            P("ep", None, "tp"),
            P("ep", None, "tp"),
            P("ep", "tp", None),
        ),
        out_specs=(P(None, "ep"), P("ep", "tp", None, None), P("ep", "tp", None), P("ep", "tp")),
        check_vma=False,
    )
```

profile of v0, /device:TPU:0, one launch (start us, length us, event | category | flops | bytes accessed | tf_op | source)
XLA Modules:
  0.0 114.8 jit_solution(4171381798939121330)
XLA Ops:
  7.2 1.4 %fusion.48 = f32[]{:T(128)} fusion(f32[4]{0:T(128)} %param.28, s32[]{:T(128)S(6)} %axis_index.12), kind=kLoop, calls=%fused_computation.81 | loop fusion | flops 11 | bytes 24 | tf_op jit(solution)/shard_map/reduce_sum | solution.py:70
  8.7 0.8 fusion.28
  9.5 0.9 fusion.3
  10.4 0.9 fusion.2
  11.3 1.3 %fusion.46 = (f32[8]{0:T(128)S(1)}, f32[8]{0:T(128)S(1)}) fusion(f32[8]{0:T(128)S(1)} %fusion.3, f32[8,1]{0,1:T(1,128)} %param.33, f32[8]{0:T(128)S(1)} %fusion.2, f32[]{:T(128)} %fusion.48), kind=kLoop, calls=%fused_computation.79 | loop fusion | flops 96 | bytes 164 | tf_op jit(solution)/shard_map/exp | solution.py:73
  12.7 1.3 %exponential_bitcast_fusion = (f32[8]{0:T(128)S(1)}, f32[8,1]{0,1:T(1,128)S(1)}) fusion(f32[8]{0:T(128)S(1)} %fusion.3, f32[8,1]{0,1:T(1,128)} %param.33, f32[8]{0:T(128)S(1)} %fusion.2, f32[]{:T(128)} %fusion.48), kind=kLoop, calls=%fused_computation.104 | loop fusion | flops 96 | bytes 164 | tf_op jit(solution)/shard_map/mul | solution.py:79
  14.1 0.9 convolution_convert_fusion.5
  14.9 1.2 %convolution_convert_fusion.4 = bf16[8,128]{1,0:T(8,128)(2,1)S(1)} fusion(bf16[1024,128]{1,0:T(8,128)(2,1)} %param.23, bf16[8,1024]{1,0:T(8,128)(2,1)S(1)} %copy-done.3, f32[1024]{0:T(1024)} %param.21, f32[8]{0:T(128)S(1)} %add_rsqrt_fusion.2), kind=kOutput, calls=%fused_computation.9 | convolution fusion | flops 2130944 | bytes 284704 | tf_op jit(solution)/shard_map/dot_general | solution.py:57
  16.1 0.9 convolution_convert_fusion.2
  17.0 1.3 %convolution_convert_fusion.3 = bf16[8,256]{1,0:T(8,128)(2,1)S(1)} fusion(bf16[1024,256]{1,0:T(8,128)(2,1)} %param.25, bf16[8,1024]{1,0:T(8,128)(2,1)S(1)} %copy-done.3, f32[1024]{0:T(1024)} %param.21, f32[8]{0:T(128)S(1)} %add_rsqrt_fusion.2), kind=kOutput, calls=%fused_computation.8 | convolution fusion | flops 4229120 | bytes 548896 | tf_op jit(solution)/shard_map/dot_general | solution.py:60
  19.0 0.8 multiply_reduce_fusion.1
  21.5 12.7 %psum.14 = bf16[8,1024]{1,0:T(8,128)(2,1)S(1)} all-reduce(bf16[8,1024]{1,0:T(8,128)(2,1)S(1)} %convolution_convert_fusion.1), channel_id=1, replica_groups=mesh['ep'=8,'tp'=4] {'tp'}, use_global_device_ids=true, to_apply=%region_6.7 | all-reduce | flops 8192 | bytes 32768 | tf_op jit(solution)/shard_map/psum | solution.py:85
  34.8 6.0 %all-to-all-start = ((bf16[8,8,128]{2,0,1:T(8,128)(2,1)}), bf16[8,8,128]{2,0,1:T(8,128)(2,1)S(1)}, u32[]{:S(2)}, u32[]{:S(2)}) async-start(bf16[8,8,128]{2,0,1:T(8,128)(2,1)} %fusion.34), calls=%async_computation | async-start | bytes 32768 | tf_op jit(solution)/shard_map/all_to_all | solution.py:89
  41.8 5.6 %all-to-all-done = bf16[8,8,128]{2,0,1:T(8,128)(2,1)S(1)} async-done(((bf16[8,8,128]{2,0,1:T(8,128)(2,1)}), bf16[8,8,128]{2,0,1:T(8,128)(2,1)S(1)}, u32[]{:S(2)}, u32[]{:S(2)}) %all-to-all-start) | async-done | bytes 16416 | tf_op jit(solution)/shard_map/all_to_all | solution.py:89
  47.4 0.9 scatter_custom_fusion
  48.3 9.3 %all_to_all.43 = bf16[8,32,128]{2,1,0:T(8,128)(2,1)S(1)} all-to-all(bf16[8,32,128]{2,1,0:T(8,128)(2,1)S(1)} %bitcast.126), channel_id=1, replica_groups=mesh['ep'=8,'tp'=4] {'ep'}, dimensions={0} | all-to-all | bytes 131072 | tf_op jit(solution)/shard_map/all_to_all | solution.py:99
  59.3 0.9 fusion
  60.3 1.2 %multiply_add_fusion = f32[8,1,128,256]{3,2,1,0:T(8,128)} fusion(f32[8,1,128,256]{3,2,1,0:T(8,128)S(1)} %copy-done.1, f32[8,256]{1,0:T(8,128)S(1)} %convert_element_type.117, f32[8,128]{1,0:T(8,128)S(1)} %get-tuple-element.30, f32[8]{0:T(128)S(1)} %get-tuple-element.24), kind=kLoop, calls=%fused_computation.18 | loop fusion | flops 786432 | bytes 2109472 | tf_op jit(solution)/shard_map/add | solution.py:76
  61.5 27.0 %all-reduce.2.cloned.1.call-done = bf16[1,32,1024]{2,1,0:T(8,128)(2,1)} async-done(((bf16[1,32,1024]{2,1,0:T(8,128)(2,1)}), bf16[1,32,1024]{2,1,0:T(8,128)(2,1)}) %all-reduce.2.cloned.1.call-update) | async-done | bytes 65552 | tf_op jit(solution)/shard_map/psum | solution.py:107
  88.5 1.1 copy.50
  90.1 2.3 %reduce.3 = bf16[1024,32]{1,0:T(8,128)(2,1)S(1)} reduce(bf16[1024,1,32]{2,1,0:T(2,128)(2,1)S(1)} %bitcast.121, bf16[]{:T(256)} %broadcast.215), dimensions={1}, to_apply=%bitcast.105.reduce_sub_computation | reduce | bytes 131074
  92.4 0.9 reshape.303
  93.3 5.5 %all-to-all-start.2 = ((bf16[8,2,2048]{2,1,0:T(2,128)(2,1)}), bf16[8,2,2048]{2,1,0:T(2,128)(2,1)S(1)}, u32[]{:S(2)}, u32[]{:S(2)}) async-start(bf16[8,2,2048]{2,1,0:T(2,128)(2,1)} %reshape.303), calls=%async_computation.2 | async-start | bytes 131072 | tf_op jit(solution)/shard_map/all_to_all | solution.py:108
  99.0 6.8 %all-to-all-done.2 = bf16[8,2,2048]{2,1,0:T(2,128)(2,1)S(1)} async-done(((bf16[8,2,2048]{2,1,0:T(2,128)(2,1)}), bf16[8,2,2048]{2,1,0:T(2,128)(2,1)S(1)}, u32[]{:S(2)}, u32[]{:S(2)}) %all-to-all-start.2) | async-done | bytes 65568 | tf_op jit(solution)/shard_map/all_to_all | solution.py:108
  (69 shorter events, 8.5 us)
Async XLA Ops:
  7.2 13.5 %copy-start = (bf16[256,1024]{1,0:T(8,128)(2,1)S(1)}, bf16[256,1024]{1,0:T(8,128)(2,1)}, u32[]{:S(2)}) copy-start(bf16[256,1024]{1,0:T(8,128)(2,1)} %param.30) | copy-start | bytes 1572868
  7.2 2.3 %copy-start.3 = (bf16[8,1024]{1,0:T(8,128)(2,1)S(1)}, bf16[8,1024]{1,0:T(8,128)(2,1)}, u32[]{:S(2)}) copy-start(bf16[8,1024]{1,0:T(8,128)(2,1)} %param.20) | copy-start | bytes 49156
  7.2 6.8 %copy-start.12 = (bf16[1024,128]{1,0:T(8,128)(2,1)S(1)}, bf16[1024,128]{1,0:T(8,128)(2,1)}, u32[]{:S(2)}) copy-start(bf16[1024,128]{1,0:T(8,128)(2,1)} %param.22) | copy-start | bytes 786436
  7.2 8.9 %copy-start.2 = (bf16[1024,256]{1,0:T(8,128)(2,1)S(1)}, bf16[1024,256]{1,0:T(8,128)(2,1)}, u32[]{:S(2)}) copy-start(bf16[1024,256]{1,0:T(8,128)(2,1)} %param.24) | copy-start | bytes 1572868
  7.2 12.6 %copy-start.1 = (f32[8,1,128,256]{3,2,1,0:T(8,128)S(1)}, f32[8,1,128,256]{3,2,1,0:T(8,128)}, u32[]{:S(2)}) copy-start(f32[8,1,128,256]{3,2,1,0:T(8,128)} %param.31) | copy-start | bytes 3145732
  14.0 5.8 %copy-start.11 = (f32[8,1]{0,1:T(1,128)}, f32[8,1]{0,1:T(1,128)S(1)}, u32[]{:S(2)}) copy-start(f32[8,1]{0,1:T(1,128)S(1)} %get-tuple-element.29) | copy-start | bytes 100
  18.3 0.7 copy-start.10
  20.6 0.7 copy-start.13
  34.8 6.0 %copy-start.8 = (s32[64,2]{0,1:T(2,128)S(1)}, s32[64,2]{0,1:T(2,128)}, u32[]{:S(2)}) copy-start(s32[64,2]{0,1:T(2,128)} %param.35) | copy-start | bytes 1540
  34.8 12.5 %all-to-all-start = ((bf16[8,8,128]{2,0,1:T(8,128)(2,1)}), bf16[8,8,128]{2,0,1:T(8,128)(2,1)S(1)}, u32[]{:S(2)}, u32[]{:S(2)}) async-start(bf16[8,8,128]{2,0,1:T(8,128)(2,1)} %fusion.34), calls=%async_computation | async-start | bytes 32768 | tf_op jit(solution)/shard_map/all_to_all | solution.py:89
  40.8 47.7 %all-reduce.2.cloned.1.call-start = ((), (), s32[]{:S(2)}) async-start(), calls=%async_computation.3 | async-start | bytes 131072 | tf_op jit(solution)/shard_map/psum | solution.py:107
  47.4 11.0 %copy-start.4 = (bf16[1,1024,128]{2,1,0:T(8,128)(2,1)S(1)}, bf16[1,1024,128]{2,1,0:T(8,128)(2,1)}, u32[]{:S(2)}) copy-start(bf16[1,1024,128]{2,1,0:T(8,128)(2,1)} %param.37) | copy-start | bytes 786436
  57.6 0.7 copy-start.7
  58.3 0.9 copy-start.6
  58.4 1.0 copy-start.5
  60.3 1.2 %copy-start.9 = (f32[64,2]{0,1:T(2,128)S(1)}, f32[64,2]{0,1:T(2,128)}, u32[]{:S(2)}) copy-start(f32[64,2]{0,1:T(2,128)} %param.36) | copy-start | bytes 1540
  93.3 12.4 %all-to-all-start.2 = ((bf16[8,2,2048]{2,1,0:T(2,128)(2,1)}), bf16[8,2,2048]{2,1,0:T(2,128)(2,1)S(1)}, u32[]{:S(2)}, u32[]{:S(2)}) async-start(bf16[8,2,2048]{2,1,0:T(2,128)(2,1)} %reshape.303), calls=%async_computation.2 | async-start | bytes 131072 | tf_op jit(solution)/shard_map/all_to_all | solution.py:108
Sparse Core Ops, SparseCore 0:
  60.4 28.0 all-reduce.1
where the time goes:
time: 116 us; the launch traced here: 115 us
  waiting for transfers between devices  39.4 us (34%)
  blocking collectives  22 us (19%)
  between operations  14.3 us (12%)
  starting transfers between devices  11.5 us (10%)
  other arithmetic  11.4 us (10%)
  local copies, waits for them, and re-layouts  8.14 us (7%)
  matrix products  7.98 us (7%)
    psum x1, waiting for transfers between devices, shards(): results = lax.psum(partial_value.astype(jnp.bfloat16), 'tp')  27 us
    psum x1, blocking collectives, shards(): lax.psum(jnp.dot(gated, w_out, preferred_element_type=jnp.float32).astype...  12.7 us
    all_to_all x1, blocking collectives, shards(): rows = lax.all_to_all(buffer, 'ep', split_axis=0, concat_axis=2, tiled=True)  9.29 us
    all_to_all x1, waiting for transfers between devices, shards(): lax.all_to_all(results, 'ep', split_axis=2, concat_axis=0, tiled=True)  6.79 us
    all_to_all x1, starting transfers between devices, shards(): lax.all_to_all(middle_rows, 'ep', split_axis=1, concat_axis=0, tiled=True)  5.97 us
    all_to_all x1, waiting for transfers between devices, shards(): lax.all_to_all(middle_rows, 'ep', split_axis=1, concat_axis=0, tiled=True)  5.58 us
    all_to_all x1, starting transfers between devices, shards(): lax.all_to_all(results, 'ep', split_axis=2, concat_axis=0, tiled=True)  5.52 us
    unnamed x33, local copies, waits for them, and re-layouts  4.59 us
  transfers between devices with their start and end apart: 3, of which 3 were waited for; matrix products, arithmetic and copies ran while one was open for 2% of the time, Pallas kernels for 0%

commit v1 on v0

--- a/solution.py
+++ b/solution.py
@@ -82,8 +82,11 @@
     read = numer / jnp.maximum(jnp.abs(denom), jnp.exp(-new_max))[:, None]
     scale = lax.rsqrt(jnp.mean(read * read, axis=-1, keepdims=True) + EPS)
     gated = (jax.nn.sigmoid(ogate) * read * scale * head_gain).astype(jnp.bfloat16)
-    local_output = lax.psum(
-        jnp.dot(gated, w_out, preferred_element_type=jnp.float32).astype(jnp.bfloat16), "tp"
+    local_output = jnp.sum(
+        lax.all_gather(
+            jnp.dot(gated, w_out, preferred_element_type=jnp.float32).astype(jnp.bfloat16), "tp"
+        ),
+        axis=0,
     ).astype(jnp.float32)
     middle_rows = (tokens.astype(jnp.float32) + local_output).astype(jnp.bfloat16)
     middle = lax.all_to_all(middle_rows, "ep", split_axis=1, concat_axis=0, tiled=True)

time: 116 us -> 111 us (0.957)
  blocking collectives: 22 us -> 15.5 us
    psum x1 -> x0, blocking collectives: 12.7 us -> none  [shards(): lax.psum(jnp.dot(gated, w_out, preferred_element_type=jnp.float32).astype...]
    all_gather x0 -> x1, blocking collectives: none -> 6.19 us  [shards(): lax.all_gather(jnp.dot(gated, w_out, preferred_element_type=jnp.float32)....]
where the time goes in v1:
time: 111 us; the launch traced here: 110 us
  waiting for transfers between devices  40.3 us (36%)
  blocking collectives  15.5 us (14%)
  between operations  14.3 us (13%)
  starting transfers between devices  12 us (11%)
  other arithmetic  11.4 us (10%)
  local copies, waits for them, and re-layouts  8.12 us (7%)
  matrix products  8 us (7%)
    psum x1, waiting for transfers between devices, shards(): results = lax.psum(partial_value.astype(jnp.bfloat16), 'tp')  27.9 us
    all_to_all x1, blocking collectives, shards(): rows = lax.all_to_all(buffer, 'ep', split_axis=0, concat_axis=2, tiled=True)  9.29 us
    all_to_all x1, waiting for transfers between devices, shards(): lax.all_to_all(results, 'ep', split_axis=2, concat_axis=0, tiled=True)  6.79 us
    all_to_all x1, starting transfers between devices, shards(): lax.all_to_all(middle_rows, 'ep', split_axis=1, concat_axis=0, tiled=True)  6.49 us
    all_gather x1, blocking collectives, shards(): lax.all_gather(jnp.dot(gated, w_out, preferred_element_type=jnp.float32)....  6.19 us
    all_to_all x1, waiting for transfers between devices, shards(): lax.all_to_all(middle_rows, 'ep', split_axis=1, concat_axis=0, tiled=True)  5.58 us
    all_to_all x1, starting transfers between devices, shards(): lax.all_to_all(results, 'ep', split_axis=2, concat_axis=0, tiled=True)  5.52 us
    unnamed x33, local copies, waits for them, and re-layouts  4.57 us
  transfers between devices with their start and end apart: 3, of which 3 were waited for; matrix products, arithmetic and copies ran while one was open for 2% of the time, Pallas kernels for 0%

profile of v1, /device:TPU:0, one launch (start us, length us, event | category | flops | bytes accessed | tf_op | source)
XLA Modules:
  0.0 109.8 jit_solution(2509092424329172171)
XLA Ops:
  7.2 1.4 %fusion.48 = f32[]{:T(128)} fusion(f32[4]{0:T(128)} %param.28, s32[]{:T(128)S(6)} %axis_index.12), kind=kLoop, calls=%fused_computation.82 | loop fusion | flops 11 | bytes 24 | tf_op jit(solution)/shard_map/reduce_sum | solution.py:70
  8.7 0.8 fusion.28
  9.5 0.9 fusion.3
  10.4 0.9 fusion.2
  11.3 1.3 %fusion.46 = (f32[8]{0:T(128)S(1)}, f32[8]{0:T(128)S(1)}) fusion(f32[8]{0:T(128)S(1)} %fusion.3, f32[8,1]{0,1:T(1,128)} %param.33, f32[8]{0:T(128)S(1)} %fusion.2, f32[]{:T(128)} %fusion.48), kind=kLoop, calls=%fused_computation.80 | loop fusion | flops 96 | bytes 164 | tf_op jit(solution)/shard_map/exp | solution.py:73
  12.7 1.3 %exponential_bitcast_fusion = (f32[8]{0:T(128)S(1)}, f32[8,1]{0,1:T(1,128)S(1)}) fusion(f32[8]{0:T(128)S(1)} %fusion.3, f32[8,1]{0,1:T(1,128)} %param.33, f32[8]{0:T(128)S(1)} %fusion.2, f32[]{:T(128)} %fusion.48), kind=kLoop, calls=%fused_computation.105 | loop fusion | flops 96 | bytes 164 | tf_op jit(solution)/shard_map/mul | solution.py:79
  14.1 0.9 convolution_convert_fusion.5
  14.9 1.2 %convolution_convert_fusion.4 = bf16[8,128]{1,0:T(8,128)(2,1)S(1)} fusion(bf16[1024,128]{1,0:T(8,128)(2,1)} %param.23, bf16[8,1024]{1,0:T(8,128)(2,1)S(1)} %copy-done.3, f32[1024]{0:T(1024)} %param.21, f32[8]{0:T(128)S(1)} %add_rsqrt_fusion.2), kind=kOutput, calls=%fused_computation.9 | convolution fusion | flops 2130944 | bytes 284704 | tf_op jit(solution)/shard_map/dot_general | solution.py:57
  16.1 0.9 convolution_convert_fusion.2
  17.0 1.3 %convolution_convert_fusion.3 = bf16[8,256]{1,0:T(8,128)(2,1)S(1)} fusion(bf16[1024,256]{1,0:T(8,128)(2,1)} %param.25, bf16[8,1024]{1,0:T(8,128)(2,1)S(1)} %copy-done.3, f32[1024]{0:T(1024)} %param.21, f32[8]{0:T(128)S(1)} %add_rsqrt_fusion.2), kind=kOutput, calls=%fused_computation.8 | convolution fusion | flops 4229120 | bytes 548896 | tf_op jit(solution)/shard_map/dot_general | solution.py:60
  19.0 0.8 multiply_reduce_fusion.1
  21.5 6.2 %all-gather = bf16[32,1024]{1,0:T(8,128)(2,1)S(1)} all-gather(bf16[8,1024]{1,0:T(8,128)(2,1)S(1)} %convolution_convert_fusion.1), channel_id=2, replica_groups=mesh['ep'=8,'tp'=4] {'tp'}, dimensions={0}, use_global_device_ids=true | all-gather | bytes 81920 | tf_op jit(solution)/shard_map/all_gather | solution.py:86
  28.3 6.5 %all-to-all-start = ((bf16[8,8,128]{2,0,1:T(8,128)(2,1)}), bf16[8,8,128]{2,0,1:T(8,128)(2,1)S(1)}, u32[]{:S(2)}, u32[]{:S(2)}) async-start(bf16[8,8,128]{2,0,1:T(8,128)(2,1)} %fusion.34), calls=%async_computation | async-start | bytes 32768 | tf_op jit(solution)/shard_map/all_to_all | solution.py:92
  35.8 5.6 %all-to-all-done = bf16[8,8,128]{2,0,1:T(8,128)(2,1)S(1)} async-done(((bf16[8,8,128]{2,0,1:T(8,128)(2,1)}), bf16[8,8,128]{2,0,1:T(8,128)(2,1)S(1)}, u32[]{:S(2)}, u32[]{:S(2)}) %all-to-all-start) | async-done | bytes 16416 | tf_op jit(solution)/shard_map/all_to_all | solution.py:92
  41.4 0.9 scatter_custom_fusion
  42.3 9.3 %all_to_all.43 = bf16[8,32,128]{2,1,0:T(8,128)(2,1)S(1)} all-to-all(bf16[8,32,128]{2,1,0:T(8,128)(2,1)S(1)} %bitcast.128), channel_id=1, replica_groups=mesh['ep'=8,'tp'=4] {'ep'}, dimensions={0} | all-to-all | bytes 131072 | tf_op jit(solution)/shard_map/all_to_all | solution.py:102
  53.4 0.9 fusion
  54.3 1.2 %multiply_add_fusion = f32[8,1,128,256]{3,2,1,0:T(8,128)} fusion(f32[8,1,128,256]{3,2,1,0:T(8,128)S(1)} %copy-done.1, f32[8,256]{1,0:T(8,128)S(1)} %convert_element_type.119, f32[8,128]{1,0:T(8,128)S(1)} %get-tuple-element.30, f32[8]{0:T(128)S(1)} %get-tuple-element.24), kind=kLoop, calls=%fused_computation.18 | loop fusion | flops 786432 | bytes 2109472 | tf_op jit(solution)/shard_map/add | solution.py:76
  55.5 27.9 %all-reduce.2.cloned.1.call-done = bf16[1,32,1024]{2,1,0:T(8,128)(2,1)} async-done(((bf16[1,32,1024]{2,1,0:T(8,128)(2,1)}), bf16[1,32,1024]{2,1,0:T(8,128)(2,1)}) %all-reduce.2.cloned.1.call-update) | async-done | bytes 65552 | tf_op jit(solution)/shard_map/psum | solution.py:110
  83.5 1.1 %copy.50 = bf16[1,32,1024]{1,0,2:T(2,128)(2,1)S(1)} copy(bf16[1,32,1024]{2,1,0:T(8,128)(2,1)} %all-reduce.2.cloned.1.call-done) | data formatting | bytes 131072 | tf_op jit(solution)/shard_map/psum | solution.py:110
  85.1 2.3 %reduce.4 = bf16[1024,32]{1,0:T(8,128)(2,1)S(1)} reduce(bf16[1024,1,32]{2,1,0:T(2,128)(2,1)S(1)} %bitcast.123, bf16[]{:T(256)} %broadcast.215), dimensions={1}, to_apply=%bitcast.107.reduce_sub_computation | reduce | bytes 131074
  87.4 0.9 reshape.304
  88.3 5.5 %all-to-all-start.2 = ((bf16[8,2,2048]{2,1,0:T(2,128)(2,1)}), bf16[8,2,2048]{2,1,0:T(2,128)(2,1)S(1)}, u32[]{:S(2)}, u32[]{:S(2)}) async-start(bf16[8,2,2048]{2,1,0:T(2,128)(2,1)} %reshape.304), calls=%async_computation.2 | async-start | bytes 131072 | tf_op jit(solution)/shard_map/all_to_all | solution.py:111
  93.9 6.8 %all-to-all-done.2 = bf16[8,2,2048]{2,1,0:T(2,128)(2,1)S(1)} async-done(((bf16[8,2,2048]{2,1,0:T(2,128)(2,1)}), bf16[8,2,2048]{2,1,0:T(2,128)(2,1)S(1)}, u32[]{:S(2)}, u32[]{:S(2)}) %all-to-all-start.2) | async-done | bytes 65568 | tf_op jit(solution)/shard_map/all_to_all | solution.py:111
  (70 shorter events, 8.6 us)
Async XLA Ops:
  7.2 13.5 %copy-start = (bf16[256,1024]{1,0:T(8,128)(2,1)S(1)}, bf16[256,1024]{1,0:T(8,128)(2,1)}, u32[]{:S(2)}) copy-start(bf16[256,1024]{1,0:T(8,128)(2,1)} %param.30) | copy-start | bytes 1572868
  7.2 2.3 %copy-start.3 = (bf16[8,1024]{1,0:T(8,128)(2,1)S(1)}, bf16[8,1024]{1,0:T(8,128)(2,1)}, u32[]{:S(2)}) copy-start(bf16[8,1024]{1,0:T(8,128)(2,1)} %param.20) | copy-start | bytes 49156
  7.2 6.8 %copy-start.12 = (bf16[1024,128]{1,0:T(8,128)(2,1)S(1)}, bf16[1024,128]{1,0:T(8,128)(2,1)}, u32[]{:S(2)}) copy-start(bf16[1024,128]{1,0:T(8,128)(2,1)} %param.22) | copy-start | bytes 786436
  7.2 8.9 %copy-start.2 = (bf16[1024,256]{1,0:T(8,128)(2,1)S(1)}, bf16[1024,256]{1,0:T(8,128)(2,1)}, u32[]{:S(2)}) copy-start(bf16[1024,256]{1,0:T(8,128)(2,1)} %param.24) | copy-start | bytes 1572868
  7.2 12.6 %copy-start.1 = (f32[8,1,128,256]{3,2,1,0:T(8,128)S(1)}, f32[8,1,128,256]{3,2,1,0:T(8,128)}, u32[]{:S(2)}) copy-start(f32[8,1,128,256]{3,2,1,0:T(8,128)} %param.31) | copy-start | bytes 3145732
  14.0 5.8 %copy-start.11 = (f32[8,1]{0,1:T(1,128)}, f32[8,1]{0,1:T(1,128)S(1)}, u32[]{:S(2)}) copy-start(f32[8,1]{0,1:T(1,128)S(1)} %get-tuple-element.29) | copy-start | bytes 100
  18.3 0.7 copy-start.10
  20.6 0.7 copy-start.13
  28.3 6.5 %copy-start.8 = (s32[64,2]{0,1:T(2,128)S(1)}, s32[64,2]{0,1:T(2,128)}, u32[]{:S(2)}) copy-start(s32[64,2]{0,1:T(2,128)} %param.35) | copy-start | bytes 1540
  28.3 13.1 %all-to-all-start = ((bf16[8,8,128]{2,0,1:T(8,128)(2,1)}), bf16[8,8,128]{2,0,1:T(8,128)(2,1)S(1)}, u32[]{:S(2)}, u32[]{:S(2)}) async-start(bf16[8,8,128]{2,0,1:T(8,128)(2,1)} %fusion.34), calls=%async_computation | async-start | bytes 32768 | tf_op jit(solution)/shard_map/all_to_all | solution.py:92
  34.8 48.7 %all-reduce.2.cloned.1.call-start = ((), (), s32[]{:S(2)}) async-start(), calls=%async_computation.3 | async-start | bytes 131072 | tf_op jit(solution)/shard_map/psum | solution.py:110
  41.4 11.0 %copy-start.4 = (bf16[1,1024,128]{2,1,0:T(8,128)(2,1)S(1)}, bf16[1,1024,128]{2,1,0:T(8,128)(2,1)}, u32[]{:S(2)}) copy-start(bf16[1,1024,128]{2,1,0:T(8,128)(2,1)} %param.37) | copy-start | bytes 786436
  51.6 0.7 copy-start.7
  52.3 0.9 copy-start.6
  52.4 1.0 copy-start.5
  54.3 1.2 %copy-start.9 = (f32[64,2]{0,1:T(2,128)S(1)}, f32[64,2]{0,1:T(2,128)}, u32[]{:S(2)}) copy-start(f32[64,2]{0,1:T(2,128)} %param.36) | copy-start | bytes 1540
  88.3 12.4 %all-to-all-start.2 = ((bf16[8,2,2048]{2,1,0:T(2,128)(2,1)}), bf16[8,2,2048]{2,1,0:T(2,128)(2,1)S(1)}, u32[]{:S(2)}, u32[]{:S(2)}) async-start(bf16[8,2,2048]{2,1,0:T(2,128)(2,1)} %reshape.304), calls=%async_computation.2 | async-start | bytes 131072 | tf_op jit(solution)/shard_map/all_to_all | solution.py:111
Sparse Core Ops, SparseCore 0:
  54.4 29.0 all-reduce.1
